TPU v7x, 256 devices: a whole 4x4x8 slice. The times are simulated.
256 devices in a mesh: sp: 32 (over z, y), dp: 8 (over x, core).
Axes of the slice: x: 4, y: 4, z: 8, core: 2. Of those that a mesh axis runs over, the one named last changes fastest.
Arguments:
- cotangent: bfloat16 [8, 8192, 4096], P('dp', 'sp'), may hold values from -6 to 6
- up_pre: bfloat16 [8, 8192, 4096], P('dp', 'sp'), may hold values from -6 to 6
- value_pre: bfloat16 [8, 8192, 4096], P('dp', 'sp'), may hold values from -6 to 6
- spatial_weight: bfloat16 [32, 1024, 1024], P('sp', 'dp'), may hold values from -0.1875 to 0.1875
- spatial_bias: float32 [32, 1024], P('sp'), may hold values from 0.5 to 1.5
- value_gain: float32 [4096], replicated, may hold values from 0.1 to 1.9
Outputs:
- up_grad: bfloat16 [8, 8192, 4096], P('dp', 'sp')
- value_grad: bfloat16 [8, 8192, 4096], P('dp', 'sp')
- weight_grad: float32 [32, 1024, 1024], P('sp', 'dp')
- bias_grad: float32 [32, 1024], P('sp', 'dp')
- gain_grad: float32 [4096], replicated
All inputs are finite; a program needn't handle non-finite values.
Results may differ from a plain program's by a relative error of at most 0.0064.
Values may be sent and summed in bfloat16 or wider, within the bound.
A program may use at most 128 MiB of HBM per device.

v0:
```python
import math
import jax
import jax.numpy as jnp
from jax import lax
from jax.sharding import Mesh
from jax.sharding import PartitionSpec as P

SP = ("sp_0", "sp_1")
DP = ("dp_0", "dp_1")
PLANE = ("dp_0", "dp_1", "sp_1")
SWAP = ("sp_0", "dp_0", "dp_1")
ALL = ("sp_0", "sp_1", "dp_0", "dp_1")
norm_floor = 0.5
root_half = 1.0 / math.sqrt(2.0)
inv_root_tau = 1.0 / math.sqrt(2.0 * math.pi)


def gelu_slope(values):
    return (
        0.5 * (1.0 + jax.scipy.special.erf(values * root_half))
        + values * jnp.exp(-0.5 * values * values) * inv_root_tau
    )


def swapped(shard, n):
    pairs = [(a * n + b, b * n + a) for a in range(n) for b in range(n)]
    return lax.ppermute(shard, SWAP, pairs)


def shards(cotangent, up_pre, value_pre, spatial_weight, spatial_bias, value_gain):
    rows, width = cotangent.shape[1:]
    block_len = spatial_weight.shape[2]
    planes = lax.axis_size("sp_0")
    seqs = lax.axis_size(DP)
    groups = lax.axis_size(PLANE)
    dim = width // groups
    weight = lax.all_gather(swapped(spatial_weight[0], planes), "sp_0", axis=0, tiled=True)
    bias = swapped(spatial_bias, planes)[0]
    grad_tok = cotangent[0].astype(jnp.float32)
    up_arg = up_pre[0].astype(jnp.float32)
    value_arg = value_pre[0].astype(jnp.float32)
    up_act = lax.optimization_barrier(jax.nn.gelu(up_arg, approximate=False).astype(jnp.bfloat16))
    value_act = jax.nn.gelu(value_arg, approximate=False)
    inv_rms = lax.rsqrt(jnp.mean(value_act * value_act, axis=-1, keepdims=True) + norm_floor)
    normed = value_act * inv_rms
    value_norm = (normed * value_gain).astype(jnp.bfloat16)
    gate_tok = (grad_tok * up_act.astype(jnp.float32)).astype(jnp.bfloat16)

    def outward(tok):
        tok = tok.reshape(rows, groups, dim).transpose(1, 0, 2)
        got = lax.all_to_all(tok, PLANE, split_axis=0, concat_axis=0, tiled=True)
        return got.reshape(seqs, block_len, dim)

    def homeward(heads):
        got = heads.reshape(groups, rows, dim)
        got = lax.all_to_all(got, PLANE, split_axis=0, concat_axis=0, tiled=True)
        return got.transpose(1, 0, 2).reshape(rows, width)

    value_blocks = outward(value_norm)
    gate_blocks = outward(gate_tok)
    back_heads = jnp.einsum(
        "pq,npc->nqc", weight, gate_blocks, preferred_element_type=jnp.float32
    ).astype(jnp.bfloat16)
    back_full = homeward(back_heads).astype(jnp.float32)
    mixed_heads = jnp.einsum(
        "pq,nqc->npc", weight, value_blocks, preferred_element_type=jnp.float32
    )
    mixed_heads = (mixed_heads + bias[None, :, None]).astype(jnp.bfloat16)
    mixed_tok = homeward(mixed_heads).astype(jnp.float32)
    weight_term = jnp.einsum(
        "npc,nqc->pq", gate_blocks, value_blocks, preferred_element_type=jnp.float32
    )
    bias_term = jnp.sum(gate_blocks, axis=(0, 2), dtype=jnp.float32)
    both = jnp.concatenate(
        [weight_term, jnp.broadcast_to(bias_term[:, None], (block_len, 128))], axis=1
    )
    both = lax.psum_scatter(both, "sp_0", scatter_dimension=0, tiled=True)
    both = swapped(both, planes)
    weight_grad = both[None, :, :block_len]
    bias_grad = both[None, :, block_len]
    up_mid = lax.optimization_barrier((grad_tok * mixed_tok).astype(jnp.bfloat16))
    up_grad = (up_mid.astype(jnp.float32) * gelu_slope(up_arg)).astype(jnp.bfloat16)[None]
    gain_grad = lax.psum(jnp.sum(back_full * normed, axis=0), ALL)
    scaled = back_full * value_gain
    value_slope = inv_rms * scaled - inv_rms**3 * value_act * jnp.mean(
        scaled * value_act, axis=-1, keepdims=True
    )
    value_grad = (value_slope * gelu_slope(value_arg)).astype(jnp.bfloat16)[None]
    return (up_grad, value_grad, weight_grad, bias_grad, gain_grad)


def solution(mesh):
    torus = Mesh(mesh.devices.reshape(8, 4, 4, 2), ("sp_0", "sp_1", "dp_0", "dp_1"))
    in_specs = (
        P(DP, SP, None),
        P(DP, SP, None),
        P(DP, SP, None),
        P(SP, DP, None),
        P(SP, None),
        P(),
    )
    out_specs = (P(DP, SP, None), P(DP, SP, None), P(SP, DP, None), P(SP, DP), P())
    return jax.shard_map(
        shards, mesh=torus, in_specs=in_specs, out_specs=out_specs, check_vma=False
    )
```

profile of v0, /device:TPU:47, one launch (start us, length us, event | category | flops | bytes accessed | tf_op | source)
XLA Modules:
  0.0 385.7 jit_solution(6176144169898661657)
XLA Ops:
  7.2 0.0 all-gather.2.cloned.1.call-start
  7.2 6.9 %collective-permute-start = (bf16[128,1024]{1,0:T(8,128)(2,1)}, bf16[128,1024]{1,0:T(8,128)(2,1)S(1)}, u32[]{:S(2)}, u32[]{:S(2)}) collective-permute-start(bf16[128,1024]{1,0:T(8,128)(2,1)} %bitcast.165), channel_id=1, source_target_pairs={{0,0},{1,32},{2,64},{3,96},{4,128},{5,160},{6,192},{7,224},{32,1},... | collective-permute-start | bytes 786440 | tf_op jit(solution)/shard_map/ppermute | solution.py:27
  14.2 3.3 copy.39
  17.5 15.1 %collective-permute-done = bf16[128,1024]{1,0:T(8,128)(2,1)S(1)} collective-permute-done((bf16[128,1024]{1,0:T(8,128)(2,1)}, bf16[128,1024]{1,0:T(8,128)(2,1)S(1)}, u32[]{:S(2)}, u32[]{:S(2)}) %collective-permute-start) | collective-permute-done | bytes 262176 | tf_op jit(solution)/shard_map/ppermute | solution.py:27
  32.6 0.7 copy-done.3
  33.3 0.0 all-gather.2.cloned.1.call-update
  33.3 10.0 %fusion.10 = bf16[256,4096]{0,1:T(8,128)(2,1)} fusion(bf16[1,256,4096]{1,2,0:T(8,128)(2,1)S(1)} %copy.39), kind=kLoop, calls=%fused_computation.29 | loop fusion | flops 69206016 | bytes 4194304 | tf_op jit(solution)/shard_map/convert_element_type | solution.py:42
  43.3 4.1 %copy.33 = bf16[1,256,4096]{1,2,0:T(8,128)(2,1)} copy(bf16[1,256,4096]{2,1,0:T(8,128)(2,1)} %param.6) | data formatting | bytes 4194304 | tf_op args[0]
  47.4 4.1 %fusion.1 = bf16[256,4096]{0,1:T(8,128)(2,1)} fusion(bf16[256,4096]{0,1:T(8,128)(2,1)} %fusion.10, bf16[1,256,4096]{1,2,0:T(8,128)(2,1)} %copy.33), kind=kLoop, calls=%fused_computation.20 | loop fusion | flops 4194304 | bytes 6291456 | tf_op jit(solution)/shard_map/convert_element_type | solution.py:47
  51.5 7.0 %all-to-all-start.2 = ((bf16[32,256,128]{1,2,0:T(8,128)(2,1)}), bf16[32,256,128]{1,2,0:T(8,128)(2,1)}, u32[]{:S(2)}, u32[]{:S(2)}) async-start(bf16[32,256,128]{1,2,0:T(8,128)(2,1)} %bitcast.155), calls=%async_computation.2 | async-start | bytes 4194304 | tf_op jit(solution)/shard_map/all_to_all | solution.py:51
  58.6 3.3 copy.34
  61.9 22.7 %all-to-all-done.2 = bf16[32,256,128]{1,2,0:T(8,128)(2,1)} async-done(((bf16[32,256,128]{1,2,0:T(8,128)(2,1)}), bf16[32,256,128]{1,2,0:T(8,128)(2,1)}, u32[]{:S(2)}, u32[]{:S(2)}) %all-to-all-start.2) | async-done | bytes 2097184 | tf_op jit(solution)/shard_map/all_to_all | solution.py:51
  84.5 4.1 %copy.40 = bf16[32,256,128]{2,1,0:T(8,128)(2,1)} copy(bf16[32,256,128]{1,2,0:T(8,128)(2,1)} %all-to-all-done.2) | data formatting | bytes 4194304 | tf_op jit(solution)/shard_map/all_to_all | solution.py:51
  88.6 6.0 %convert_bitcast_fusion.1 = bf16[8,1024,128]{1,2,0:T(8,128)(2,1)} fusion(bf16[8,1024,128]{2,1,0:T(8,128)(2,1)} %bitcast.158, bf16[1024,1024]{1,0:T(8,128)(2,1)} %all-gather.2.cloned.1.call-done), kind=kOutput, calls=%fused_computation.165 | convolution fusion | flops 2148532224 | bytes 6291456 | tf_op jit(solution)/shard_map/pq,npc->nqc/dot_general | solution.py:61
  94.5 3.9 %copy.42 = bf16[8,1024,128]{2,1,0:T(8,128)(2,1)} copy(bf16[8,1024,128]{1,2,0:T(8,128)(2,1)} %convert_bitcast_fusion.1) | data formatting | bytes 4194304 | tf_op jit(solution)/shard_map/convert_element_type | solution.py:63
  98.5 4.1 %copy.43 = bf16[32,256,128]{1,2,0:T(8,128)(2,1)} copy(bf16[32,256,128]{2,1,0:T(8,128)(2,1)} %bitcast.157) | data formatting | bytes 4194304 | tf_op jit(solution)/shard_map/reshape | solution.py:55
  102.5 7.5 %all-to-all-start.3 = ((bf16[32,256,128]{1,2,0:T(8,128)(2,1)}), bf16[32,256,128]{1,2,0:T(8,128)(2,1)}, u32[]{:S(2)}, u32[]{:S(2)}) async-start(bf16[32,256,128]{1,2,0:T(8,128)(2,1)} %copy.43), calls=%async_computation.3 | async-start | bytes 4194304 | tf_op jit(solution)/shard_map/all_to_all | solution.py:56
  110.0 9.4 %fusion.7 = f32[256]{0:T(256)S(1)} fusion(bf16[1,256,4096]{1,2,0:T(8,128)(2,1)S(1)} %copy.34), kind=kLoop, calls=%fused_computation.26 | loop fusion | flops 70254336 | bytes 2098176 | tf_op jit(solution)/shard_map/reduce_sum | solution.py:44
  119.4 3.8 fusion.18
  123.2 12.8 %all-to-all-done.3 = bf16[32,256,128]{1,2,0:T(8,128)(2,1)} async-done(((bf16[32,256,128]{1,2,0:T(8,128)(2,1)}), bf16[32,256,128]{1,2,0:T(8,128)(2,1)}, u32[]{:S(2)}, u32[]{:S(2)}) %all-to-all-start.3) | async-done | bytes 2097184 | tf_op jit(solution)/shard_map/all_to_all | solution.py:56
  136.0 11.6 %fusion.61 = (f32[32,128]{1,0:T(8,128)S(1)}, f32[256]{0:T(256)S(1)}, f32[256,32,128]{0,2,1:T(8,128)S(1)}) fusion(bf16[32,256,128]{1,2,0:T(8,128)(2,1)} %all-to-all-done.3, f32[256]{0:T(256)S(1)} %get-tuple-element.31, f32[32,128]{1,0:T(8,128)S(1)} %bitcast.162, f32[256,32,128]{0,2,1:T(8,128)} %bitcast.154, f32[256,32,128]{0,2,1:T(8,128)} %bitcast.153), kind=kLoop, calls=%fused_computation.83 | loop fusion | flops 71298816 | bytes 14714880 | tf_op jit(solution)/shard_map/reduce_sum | solution.py:83
  147.6 1.7 fusion.121
  149.3 7.5 %all-to-all-start = ((bf16[32,256,128]{1,2,0:T(8,128)(2,1)}), bf16[32,256,128]{1,2,0:T(8,128)(2,1)}, u32[]{:S(2)}, u32[]{:S(2)}) async-start(bf16[32,256,128]{1,2,0:T(8,128)(2,1)} %fusion.121), calls=%async_computation | async-start | bytes 4194304 | tf_op jit(solution)/shard_map/all_to_all | solution.py:51
  156.8 0.2 reduce-scatter.2.cloned.1.call-start
  157.0 2.0 convert_reduce_fusion
  159.0 23.7 %all-to-all-done = bf16[32,256,128]{1,2,0:T(8,128)(2,1)} async-done(((bf16[32,256,128]{1,2,0:T(8,128)(2,1)}), bf16[32,256,128]{1,2,0:T(8,128)(2,1)}, u32[]{:S(2)}, u32[]{:S(2)}) %all-to-all-start) | async-done | bytes 2097184 | tf_op jit(solution)/shard_map/all_to_all | solution.py:51
  182.7 4.1 %copy.35 = bf16[32,256,128]{2,1,0:T(8,128)(2,1)} copy(bf16[32,256,128]{1,2,0:T(8,128)(2,1)} %all-to-all-done) | data formatting | bytes 4194304 | tf_op jit(solution)/shard_map/all_to_all | solution.py:51
  186.8 4.6 %convolution_bitcast_fusion = f32[1024,1024]{0,1:T(8,128)S(1)} fusion(bf16[8,1024,128]{2,1,0:T(8,128)(2,1)} %bitcast.159, bf16[8,1024,128]{2,1,0:T(8,128)(2,1)} %bitcast.160), kind=kOutput, calls=%fused_computation.158 | convolution fusion | flops 2147483648 | bytes 8388608 | tf_op jit(solution)/shard_map/npc,nqc->pq/dot_general | solution.py:70
  191.4 2.5 pad_maximum_fusion
  193.9 0.0 reduce-scatter.2.cloned.1.call-update
  194.0 0.7 copy-done.6
  194.6 5.6 %collective-permute-start.1 = (f32[1,1024]{1,0:T(1,128)S(1)}, f32[1,1024]{1,0:T(1,128)S(1)}, u32[]{:S(2)}, u32[]{:S(2)}) collective-permute-start(f32[1,1024]{1,0:T(1,128)S(1)} %copy-done.6), channel_id=1, source_target_pairs={{0,0},{1,32},{2,64},{3,96},{4,128},{5,160},{6,192},{7,224},{32,1},... | collective-permute-start | bytes 12296 | tf_op jit(solution)/shard_map/ppermute | solution.py:27
  200.2 4.1 %convert_element_type.124 = f32[32,256,128]{1,2,0:T(8,128)} convert(bf16[32,256,128]{1,2,0:T(8,128)(2,1)} %all-to-all-done.3) | non-fusion elementwise | flops 1048576 | bytes 6291456 | tf_op jit(solution)/shard_map/convert_element_type | solution.py:64
  204.4 3.7 fusion.122
  208.1 3.9 %copy.37 = bf16[8,1024,128]{2,1,0:T(8,128)(2,1)} copy(bf16[8,1024,128]{1,2,0:T(8,128)(2,1)} %fusion.122) | data formatting | bytes 4194304 | tf_op jit(solution)/shard_map/convert_element_type | solution.py:68
  212.0 8.6 %all-to-all-start.1 = ((bf16[32,256,128]{2,1,0:T(8,128)(2,1)}), bf16[32,256,128]{2,1,0:T(8,128)(2,1)}, u32[]{:S(2)}, u32[]{:S(2)}) async-start(bf16[32,256,128]{2,1,0:T(8,128)(2,1)} %bitcast.156), calls=%async_computation.1 | async-start | bytes 4194304 | tf_op jit(solution)/shard_map/all_to_all | solution.py:56
  220.6 15.5 %fusion.17 = bf16[1,256,4096]{1,2,0:T(8,128)(2,1)} fusion(bf16[1,256,4096]{1,2,0:T(8,128)(2,1)S(1)} %copy.34, f32[256]{0:T(256)S(1)} %broadcast_multiply_fusion, f32[256]{0:T(256)S(1)} %get-tuple-element.30, f32[4096]{0:T(1024)S(1)} %copy-done.4, f32[256]{0:T(256)S(1)} %get-tuple-element.31, f32[1,256,4096]{1,2,0:T(8,128)} %bitcast.152), kind=kLoop, calls=%fused_computation.36 | loop fusion | flops 83886080 | bytes 8408064 | tf_op jit(solution)/shard_map/convert_element_type | solution.py:88
  236.2 4.1 %copy.45 = bf16[1,256,4096]{2,1,0:T(8,128)(2,1)} copy(bf16[1,256,4096]{1,2,0:T(8,128)(2,1)} %fusion.17) | data formatting | bytes 4194304
  240.2 76.8 %psum.7 = f32[4096]{0:T(1024)} all-reduce(f32[4096]{0:T(1024)S(1)} %bitcast.164), channel_id=1, replica_groups=mesh['sp_0'=8,'sp_1'=4,'dp_0'=4,'dp_1'=2] {'sp_0','sp_1','dp_0','dp_1'}, use_global_device_ids=true, to_apply=%region_6.7 | all-reduce | flops 4096 | bytes 32768 | tf_op jit(solution)/shard_map/psum | solution.py:83
  317.0 4.1 %convert_bitcast_fusion = f32[256,32,128]{2,0,1:T(8,128)} fusion(bf16[32,256,128]{2,1,0:T(8,128)(2,1)} %all-to-all-done.1), kind=kLoop, calls=%fused_computation.140 | loop fusion | flops 1048576 | bytes 6291456 | tf_op jit(solution)/shard_map/convert_element_type | solution.py:69
  321.1 5.7 %copy.38 = f32[256,32,128]{0,2,1:T(8,128)} copy(f32[256,32,128]{2,0,1:T(8,128)} %convert_bitcast_fusion) | data formatting | bytes 8388608 | tf_op jit(solution)/shard_map/convert_element_type | solution.py:69
  326.8 4.8 %fusion = bf16[256,4096]{0,1:T(8,128)(2,1)} fusion(f32[256,32,128]{0,2,1:T(8,128)} %copy.38, bf16[1,256,4096]{1,2,0:T(8,128)(2,1)} %copy.33), kind=kLoop, calls=%fused_computation.19 | loop fusion | flops 3145728 | bytes 8388608 | tf_op jit(solution)/shard_map/convert_element_type | solution.py:81
  331.6 3.9 %collective-permute-start.2 = (f32[128,1152]{0,1:T(8,128)}, f32[128,1152]{0,1:T(8,128)S(1)}, u32[]{:S(2)}, u32[]{:S(2)}) collective-permute-start(f32[128,1152]{0,1:T(8,128)} %reduce-scatter.2.cloned.1.call-done), channel_id=1, source_target_pairs={{0,0},{1,32},{2,64},{3,96},{4,128},{5,160},{6,192},{7,224},{32,1},... | collective-permute-start | bytes 1769480 | tf_op jit(solution)/shard_map/ppermute | solution.py:27
  335.5 4.2 %fusion.127 = bf16[1,256,4096]{1,2,0:T(8,128)(2,1)} fusion(bf16[1,256,4096]{1,2,0:T(8,128)(2,1)S(1)} %copy-done.1, bf16[256,4096]{0,1:T(8,128)(2,1)} %fusion), kind=kLoop, calls=%fused_computation.166 | loop fusion | flops 12582912 | bytes 6291456 | tf_op jit(solution)/shard_map/broadcast_in_dim | solution.py:82
  339.7 4.1 %copy.44 = bf16[1,256,4096]{2,1,0:T(8,128)(2,1)} copy(bf16[1,256,4096]{1,2,0:T(8,128)(2,1)} %fusion.127) | data formatting | bytes 4194304
  343.8 33.5 %collective-permute-done.2 = f32[128,1152]{0,1:T(8,128)S(1)} collective-permute-done((f32[128,1152]{0,1:T(8,128)}, f32[128,1152]{0,1:T(8,128)S(1)}, u32[]{:S(2)}, u32[]{:S(2)}) %collective-permute-start.2) | collective-permute-done | bytes 589856 | tf_op jit(solution)/shard_map/ppermute | solution.py:27
  377.4 1.0 copy.46
  378.4 0.5 slice_bitcast_fusion.1
  (22 shorter events, 0.2 us)
Async XLA Ops:
  7.2 81.4 %all-gather.2.cloned.1.call-start = ((), (), s32[]{:S(2)}) async-start(), calls=%async_computation.5 | async-start | bytes 2359296 | tf_op jit(solution)/shard_map/all_gather | solution.py:37
  7.2 25.4 %collective-permute-start = (bf16[128,1024]{1,0:T(8,128)(2,1)}, bf16[128,1024]{1,0:T(8,128)(2,1)S(1)}, u32[]{:S(2)}, u32[]{:S(2)}) collective-permute-start(bf16[128,1024]{1,0:T(8,128)(2,1)} %bitcast.165), channel_id=1, source_target_pairs={{0,0},{1,32},{2,64},{3,96},{4,128},{5,160},{6,192},{7,224},{32,1},... | collective-permute-start | bytes 786440 | tf_op jit(solution)/shard_map/ppermute | solution.py:27
  17.4 30.0 %copy-start = (bf16[1,256,4096]{1,2,0:T(8,128)(2,1)}, bf16[1,256,4096]{1,2,0:T(8,128)(2,1)S(1)}, u32[]{:S(2)}) copy-start(bf16[1,256,4096]{1,2,0:T(8,128)(2,1)S(1)} %copy.39) | copy-start | bytes 6291460
  32.6 0.7 copy-start.3
  51.5 33.0 %all-to-all-start.2 = ((bf16[32,256,128]{1,2,0:T(8,128)(2,1)}), bf16[32,256,128]{1,2,0:T(8,128)(2,1)}, u32[]{:S(2)}, u32[]{:S(2)}) async-start(bf16[32,256,128]{1,2,0:T(8,128)(2,1)} %bitcast.155), calls=%async_computation.2 | async-start | bytes 4194304 | tf_op jit(solution)/shard_map/all_to_all | solution.py:51
  102.5 33.5 %all-to-all-start.3 = ((bf16[32,256,128]{1,2,0:T(8,128)(2,1)}), bf16[32,256,128]{1,2,0:T(8,128)(2,1)}, u32[]{:S(2)}, u32[]{:S(2)}) async-start(bf16[32,256,128]{1,2,0:T(8,128)(2,1)} %copy.43), calls=%async_computation.3 | async-start | bytes 4194304 | tf_op jit(solution)/shard_map/all_to_all | solution.py:56
  119.4 16.6 %copy-start.4 = (f32[4096]{0:T(1024)S(1)}, f32[4096]{0:T(1024)}, u32[]{:S(2)}) copy-start(f32[4096]{0:T(1024)} %param.11) | copy-start | bytes 49156
  149.3 33.5 %all-to-all-start = ((bf16[32,256,128]{1,2,0:T(8,128)(2,1)}), bf16[32,256,128]{1,2,0:T(8,128)(2,1)}, u32[]{:S(2)}, u32[]{:S(2)}) async-start(bf16[32,256,128]{1,2,0:T(8,128)(2,1)} %fusion.121), calls=%async_computation | async-start | bytes 4194304 | tf_op jit(solution)/shard_map/all_to_all | solution.py:51
  156.8 174.8 %reduce-scatter.2.cloned.1.call-start = ((), (), s32[]{:S(2)}) async-start(), calls=%async_computation.6 | async-start | bytes 5308416 | tf_op jit(solution)/shard_map/reduce_scatter | solution.py:77
  193.9 0.7 copy-start.6
  194.6 9.8 %copy-start.2 = (bf16[32,256,128]{2,1,0:T(8,128)(2,1)S(1)}, bf16[32,256,128]{2,1,0:T(8,128)(2,1)}, u32[]{:S(2)}) copy-start(bf16[32,256,128]{2,1,0:T(8,128)(2,1)} %copy.35) | copy-start | bytes 6291460
  194.6 9.8 %copy-start.5 = (bf16[1024,1024]{1,0:T(8,128)(2,1)S(1)}, bf16[1024,1024]{1,0:T(8,128)(2,1)}, u32[]{:S(2)}) copy-start(bf16[1024,1024]{1,0:T(8,128)(2,1)} %all-gather.2.cloned.1.call-done) | copy-start | bytes 6291460
  194.6 9.8 %collective-permute-start.1 = (f32[1,1024]{1,0:T(1,128)S(1)}, f32[1,1024]{1,0:T(1,128)S(1)}, u32[]{:S(2)}, u32[]{:S(2)}) collective-permute-start(f32[1,1024]{1,0:T(1,128)S(1)} %copy-done.6), channel_id=1, source_target_pairs={{0,0},{1,32},{2,64},{3,96},{4,128},{5,160},{6,192},{7,224},{32,1},... | collective-permute-start | bytes 12296 | tf_op jit(solution)/shard_map/ppermute | solution.py:27
  212.0 105.0 %all-to-all-start.1 = ((bf16[32,256,128]{2,1,0:T(8,128)(2,1)}), bf16[32,256,128]{2,1,0:T(8,128)(2,1)}, u32[]{:S(2)}, u32[]{:S(2)}) async-start(bf16[32,256,128]{2,1,0:T(8,128)(2,1)} %bitcast.156), calls=%async_computation.1 | async-start | bytes 4194304 | tf_op jit(solution)/shard_map/all_to_all | solution.py:56
  326.8 8.7 %copy-start.1 = (bf16[1,256,4096]{1,2,0:T(8,128)(2,1)S(1)}, bf16[1,256,4096]{1,2,0:T(8,128)(2,1)}, u32[]{:S(2)}) copy-start(bf16[1,256,4096]{1,2,0:T(8,128)(2,1)} %copy-done) | copy-start | bytes 6291460
  331.6 45.7 %collective-permute-start.2 = (f32[128,1152]{0,1:T(8,128)}, f32[128,1152]{0,1:T(8,128)S(1)}, u32[]{:S(2)}, u32[]{:S(2)}) collective-permute-start(f32[128,1152]{0,1:T(8,128)} %reduce-scatter.2.cloned.1.call-done), channel_id=1, source_target_pairs={{0,0},{1,32},{2,64},{3,96},{4,128},{5,160},{6,192},{7,224},{32,1},... | collective-permute-start | bytes 1769480 | tf_op jit(solution)/shard_map/ppermute | solution.py:27
Sparse Core Ops, SparseCore 0:
  33.4 36.1 all-gather.1
  194.1 58.9 reduce-scatter.1
where the time goes:
time: 387 us; the launch traced here: 386 us
  waiting for transfers between devices  108 us (28%)
  other arithmetic  77.7 us (20%)
  blocking collectives  76.8 us (20%)
  local copies, waits for them, and re-layouts  47.5 us (12%)
  starting transfers between devices  47.3 us (12%)
  matrix products  14.2 us (4%)
  between operations  14.2 us (4%)
    psum x1, blocking collectives, shards(): gain_grad = lax.psum(jnp.sum(back_full * normed, axis=0), ALL)  76.8 us
    ppermute x3, waiting for transfers between devices, swapped(): return lax.ppermute(shard, SWAP, pairs)  48.7 us
    all_to_all x2, waiting for transfers between devices, outward(): got = lax.all_to_all(tok, PLANE, split_axis=0, concat_axis=0, tiled=True)  46.4 us
    unnamed x20, local copies, waits for them, and re-layouts  21.2 us
    ppermute x3, starting transfers between devices, swapped(): return lax.ppermute(shard, SWAP, pairs)  16.5 us
    all_to_all x2, starting transfers between devices, homeward(): got = lax.all_to_all(got, PLANE, split_axis=0, concat_axis=0, tiled=True)  16.1 us
    convert_element_type x1, other arithmetic, shards(): (value_slope * gelu_slope(value_arg)).astype(jnp.bfloat16)[None]  15.5 us
    all_to_all x2, starting transfers between devices, outward(): got = lax.all_to_all(tok, PLANE, split_axis=0, concat_axis=0, tiled=True)  14.5 us
  transfers between devices with their start and end apart: 9, of which 5 were waited for; matrix products, arithmetic and copies ran while one was open for 25% of the time, Pallas kernels for 0%

commit v1 on v0

--- a/solution.py
+++ b/solution.py
@@ -80,7 +80,7 @@
     bias_grad = both[None, :, block_len]
     up_mid = lax.optimization_barrier((grad_tok * mixed_tok).astype(jnp.bfloat16))
     up_grad = (up_mid.astype(jnp.float32) * gelu_slope(up_arg)).astype(jnp.bfloat16)[None]
-    gain_grad = lax.psum(jnp.sum(back_full * normed, axis=0), ALL)
+    gain_grad = jnp.sum(lax.all_gather(jnp.sum(back_full * normed, axis=0), ALL), axis=0)
     scaled = back_full * value_gain
     value_slope = inv_rms * scaled - inv_rms**3 * value_act * jnp.mean(
         scaled * value_act, axis=-1, keepdims=True

time: 387 us -> 406 us (1.049)
  waiting for transfers between devices: 108 us -> 196 us
  blocking collectives: 76.8 us -> 0 us
  other arithmetic: 77.7 us -> 83.3 us
    all_gather x0 -> x1, waiting for transfers between devices: none -> 114 us  [shards(): lax.all_gather(jnp.sum(back_full * normed, axis=0), ALL)]
    psum x1 -> x0, blocking collectives: 76.8 us -> none  [shards(): gain_grad = lax.psum(jnp.sum(back_full * normed, axis=0), ALL)]
    ppermute x3, waiting for transfers between devices: 48.7 us -> 15.1 us  [swapped(): return lax.ppermute(shard, SWAP, pairs)]
    all_to_all x2, waiting for transfers between devices: 12.8 us -> 19.2 us  [homeward(): got = lax.all_to_all(got, PLANE, split_axis=0, concat_axis=0, tiled=True)]
    reduce_sum x1 -> x2, other arithmetic: 11.6 us -> 17.2 us  [the longest x1 12.2 us: shards(): jnp.sum(back_full * normed, axis=0)]
  transfers between devices with their start and end apart: 9 -> 10, of which waited for: 5 -> 6; matrix products, arithmetic and copies ran while one was open for 25% -> 26% of each run, Pallas kernels for 0% -> 0%
where the time goes in v1:
time: 406 us; the launch traced here: 401 us
  waiting for transfers between devices  196 us (48%)
  other arithmetic  83.3 us (21%)
  starting transfers between devices  47.1 us (12%)
  local copies, waits for them, and re-layouts  46.9 us (12%)
  matrix products  14.2 us (3%)
  between operations  13.9 us (3%)
    all_gather x1, waiting for transfers between devices, shards(): lax.all_gather(jnp.sum(back_full * normed, axis=0), ALL)  114 us
    all_to_all x2, waiting for transfers between devices, outward(): got = lax.all_to_all(tok, PLANE, split_axis=0, concat_axis=0, tiled=True)  46.4 us
    unnamed x20, local copies, waits for them, and re-layouts  20.5 us
    all_to_all x2, waiting for transfers between devices, homeward(): got = lax.all_to_all(got, PLANE, split_axis=0, concat_axis=0, tiled=True)  19.2 us
    ppermute x3, starting transfers between devices, swapped(): return lax.ppermute(shard, SWAP, pairs)  16.2 us
    all_to_all x2, starting transfers between devices, homeward(): got = lax.all_to_all(got, PLANE, split_axis=0, concat_axis=0, tiled=True)  16.1 us
    convert_element_type x1, other arithmetic, shards(): (value_slope * gelu_slope(value_arg)).astype(jnp.bfloat16)[None]  15.5 us
    ppermute x3, waiting for transfers between devices, swapped(): return lax.ppermute(shard, SWAP, pairs)  15.1 us
  transfers between devices with their start and end apart: 10, of which 6 were waited for; matrix products, arithmetic and copies ran while one was open for 26% of the time, Pallas kernels for 0%

profile of v1, /device:TPU:47, one launch (start us, length us, event | category | flops | bytes accessed | tf_op | source)
XLA Modules:
  0.0 401.4 jit_solution(1731284533966795312)
XLA Ops:
  7.2 0.0 all-gather.4.cloned.1.call-start
  7.2 6.9 %collective-permute-start = (bf16[128,1024]{1,0:T(8,128)(2,1)}, bf16[128,1024]{1,0:T(8,128)(2,1)S(1)}, u32[]{:S(2)}, u32[]{:S(2)}) collective-permute-start(bf16[128,1024]{1,0:T(8,128)(2,1)} %bitcast.165), channel_id=1, source_target_pairs={{0,0},{1,32},{2,64},{3,96},{4,128},{5,160},{6,192},{7,224},{32,1},... | collective-permute-start | bytes 786440 | tf_op jit(solution)/shard_map/ppermute | solution.py:27
  14.2 3.3 copy.53
  17.5 15.1 %collective-permute-done = bf16[128,1024]{1,0:T(8,128)(2,1)S(1)} collective-permute-done((bf16[128,1024]{1,0:T(8,128)(2,1)}, bf16[128,1024]{1,0:T(8,128)(2,1)S(1)}, u32[]{:S(2)}, u32[]{:S(2)}) %collective-permute-start) | collective-permute-done | bytes 262176 | tf_op jit(solution)/shard_map/ppermute | solution.py:27
  32.6 0.7 copy-done.3
  33.3 10.0 %fusion.10 = bf16[256,4096]{0,1:T(8,128)(2,1)} fusion(bf16[1,256,4096]{1,2,0:T(8,128)(2,1)S(1)} %copy.53), kind=kLoop, calls=%fused_computation.29 | loop fusion | flops 69206016 | bytes 4194304 | tf_op jit(solution)/shard_map/convert_element_type | solution.py:42
  43.3 4.1 %copy.47 = bf16[1,256,4096]{1,2,0:T(8,128)(2,1)} copy(bf16[1,256,4096]{2,1,0:T(8,128)(2,1)} %param.6) | data formatting | bytes 4194304 | tf_op args[0]
  47.4 4.1 %fusion.1 = bf16[256,4096]{0,1:T(8,128)(2,1)} fusion(bf16[256,4096]{0,1:T(8,128)(2,1)} %fusion.10, bf16[1,256,4096]{1,2,0:T(8,128)(2,1)} %copy.47), kind=kLoop, calls=%fused_computation.20 | loop fusion | flops 4194304 | bytes 6291456 | tf_op jit(solution)/shard_map/convert_element_type | solution.py:47
  51.5 7.0 %all-to-all-start.2 = ((bf16[32,256,128]{1,2,0:T(8,128)(2,1)}), bf16[32,256,128]{1,2,0:T(8,128)(2,1)}, u32[]{:S(2)}, u32[]{:S(2)}) async-start(bf16[32,256,128]{1,2,0:T(8,128)(2,1)} %bitcast.155), calls=%async_computation.2 | async-start | bytes 4194304 | tf_op jit(solution)/shard_map/all_to_all | solution.py:51
  58.6 3.3 copy.48
  61.8 22.7 %all-to-all-done.2 = bf16[32,256,128]{1,2,0:T(8,128)(2,1)} async-done(((bf16[32,256,128]{1,2,0:T(8,128)(2,1)}), bf16[32,256,128]{1,2,0:T(8,128)(2,1)}, u32[]{:S(2)}, u32[]{:S(2)}) %all-to-all-start.2) | async-done | bytes 2097184 | tf_op jit(solution)/shard_map/all_to_all | solution.py:51
  84.5 4.1 %copy.54 = bf16[32,256,128]{2,1,0:T(8,128)(2,1)} copy(bf16[32,256,128]{1,2,0:T(8,128)(2,1)} %all-to-all-done.2) | data formatting | bytes 4194304 | tf_op jit(solution)/shard_map/all_to_all | solution.py:51
  88.6 5.9 %convert_bitcast_fusion.1 = bf16[8,1024,128]{1,2,0:T(8,128)(2,1)} fusion(bf16[8,1024,128]{2,1,0:T(8,128)(2,1)} %bitcast.158, bf16[1024,1024]{1,0:T(8,128)(2,1)} %all-gather.4.cloned.1.call-done), kind=kOutput, calls=%fused_computation.165 | convolution fusion | flops 2148532224 | bytes 6291456 | tf_op jit(solution)/shard_map/pq,npc->nqc/dot_general | solution.py:61
  94.5 3.9 copy.56
  98.4 4.1 %copy.57 = bf16[32,256,128]{1,2,0:T(8,128)(2,1)} copy(bf16[32,256,128]{2,1,0:T(8,128)(2,1)} %bitcast.157) | data formatting | bytes 4194304 | tf_op jit(solution)/shard_map/reshape | solution.py:55
  102.5 7.5 %all-to-all-start.3 = ((bf16[32,256,128]{1,2,0:T(8,128)(2,1)}), bf16[32,256,128]{1,2,0:T(8,128)(2,1)}, u32[]{:S(2)}, u32[]{:S(2)}) async-start(bf16[32,256,128]{1,2,0:T(8,128)(2,1)} %copy.57), calls=%async_computation.3 | async-start | bytes 4194304 | tf_op jit(solution)/shard_map/all_to_all | solution.py:56
  110.0 9.4 %fusion.7 = f32[256]{0:T(256)S(1)} fusion(bf16[1,256,4096]{1,2,0:T(8,128)(2,1)S(1)} %copy.48), kind=kLoop, calls=%fused_computation.26 | loop fusion | flops 70254336 | bytes 2098176 | tf_op jit(solution)/shard_map/reduce_sum | solution.py:44
  119.4 3.8 fusion.18
  123.2 12.8 %all-to-all-done.3 = bf16[32,256,128]{1,2,0:T(8,128)(2,1)} async-done(((bf16[32,256,128]{1,2,0:T(8,128)(2,1)}), bf16[32,256,128]{1,2,0:T(8,128)(2,1)}, u32[]{:S(2)}, u32[]{:S(2)}) %all-to-all-start.3) | async-done | bytes 2097184 | tf_op jit(solution)/shard_map/all_to_all | solution.py:56
  136.0 12.2 %fusion.61 = (f32[32,128]{1,0:T(8,128)}, f32[256]{0:T(256)S(1)}, f32[256,32,128]{0,2,1:T(8,128)S(1)}) fusion(bf16[32,256,128]{1,2,0:T(8,128)(2,1)} %all-to-all-done.3, f32[256]{0:T(256)S(1)} %get-tuple-element.36, f32[32,128]{1,0:T(8,128)S(1)} %bitcast.162, f32[256,32,128]{0,2,1:T(8,128)} %bitcast.154, f32[256,32,128]{0,2,1:T(8,128)} %bitcast.153), kind=kLoop, calls=%fused_computation.83 | loop fusion | flops 71298816 | bytes 14714880 | tf_op jit(solution)/shard_map/reduce_sum | solution.py:83
  148.1 1.7 fusion.121
  149.9 7.5 %all-to-all-start = ((bf16[32,256,128]{1,2,0:T(8,128)(2,1)}), bf16[32,256,128]{1,2,0:T(8,128)(2,1)}, u32[]{:S(2)}, u32[]{:S(2)}) async-start(bf16[32,256,128]{1,2,0:T(8,128)(2,1)} %fusion.121), calls=%async_computation | async-start | bytes 4194304 | tf_op jit(solution)/shard_map/all_to_all | solution.py:51
  157.4 0.2 reduce-scatter.2.cloned.1.call-start
  157.6 2.0 convert_reduce_fusion
  159.6 23.7 %all-to-all-done = bf16[32,256,128]{1,2,0:T(8,128)(2,1)} async-done(((bf16[32,256,128]{1,2,0:T(8,128)(2,1)}), bf16[32,256,128]{1,2,0:T(8,128)(2,1)}, u32[]{:S(2)}, u32[]{:S(2)}) %all-to-all-start) | async-done | bytes 2097184 | tf_op jit(solution)/shard_map/all_to_all | solution.py:51
  183.3 4.1 %copy.49 = bf16[32,256,128]{2,1,0:T(8,128)(2,1)} copy(bf16[32,256,128]{1,2,0:T(8,128)(2,1)} %all-to-all-done) | data formatting | bytes 4194304 | tf_op jit(solution)/shard_map/all_to_all | solution.py:51
  187.4 4.6 %convolution_bitcast_fusion = f32[1024,1024]{0,1:T(8,128)S(1)} fusion(bf16[8,1024,128]{2,1,0:T(8,128)(2,1)} %bitcast.159, bf16[8,1024,128]{2,1,0:T(8,128)(2,1)} %bitcast.160), kind=kOutput, calls=%fused_computation.158 | convolution fusion | flops 2147483648 | bytes 8388608 | tf_op jit(solution)/shard_map/npc,nqc->pq/dot_general | solution.py:70
  192.0 2.5 pad_maximum_fusion
  194.6 0.0 all-gather.6.cloned.1.call-start
  194.6 0.7 all-gather.6.cloned.1.call-update
  195.3 5.6 %collective-permute-start.1 = (f32[1,1024]{1,0:T(1,128)S(1)}, f32[1,1024]{1,0:T(1,128)S(1)}, u32[]{:S(2)}, u32[]{:S(2)}) collective-permute-start(f32[1,1024]{1,0:T(1,128)S(1)} %copy-done.6), channel_id=1, source_target_pairs={{0,0},{1,32},{2,64},{3,96},{4,128},{5,160},{6,192},{7,224},{32,1},... | collective-permute-start | bytes 12296 | tf_op jit(solution)/shard_map/ppermute | solution.py:27
  201.0 4.1 %convert_element_type.124 = f32[32,256,128]{1,2,0:T(8,128)} convert(bf16[32,256,128]{1,2,0:T(8,128)(2,1)} %all-to-all-done.3) | non-fusion elementwise | flops 1048576 | bytes 6291456 | tf_op jit(solution)/shard_map/convert_element_type | solution.py:64
  205.1 3.7 fusion.122
  208.8 3.9 copy.51
  212.7 8.6 %all-to-all-start.1 = ((bf16[32,256,128]{2,1,0:T(8,128)(2,1)}), bf16[32,256,128]{2,1,0:T(8,128)(2,1)}, u32[]{:S(2)}, u32[]{:S(2)}) async-start(bf16[32,256,128]{2,1,0:T(8,128)(2,1)} %bitcast.156), calls=%async_computation.1 | async-start | bytes 4194304 | tf_op jit(solution)/shard_map/all_to_all | solution.py:56
  221.3 15.5 %fusion.17 = bf16[1,256,4096]{1,2,0:T(8,128)(2,1)} fusion(bf16[1,256,4096]{1,2,0:T(8,128)(2,1)S(1)} %copy.48, f32[256]{0:T(256)S(1)} %broadcast_multiply_fusion, f32[256]{0:T(256)S(1)} %get-tuple-element.35, f32[4096]{0:T(1024)S(1)} %copy-done.4, f32[256]{0:T(256)S(1)} %get-tuple-element.36, f32[1,256,4096]{1,2,0:T(8,128)} %bitcast.152), kind=kLoop, calls=%fused_computation.36 | loop fusion | flops 83886080 | bytes 8408064 | tf_op jit(solution)/shard_map/convert_element_type | solution.py:88
  236.9 4.1 %copy.59 = bf16[1,256,4096]{2,1,0:T(8,128)(2,1)} copy(bf16[1,256,4096]{1,2,0:T(8,128)(2,1)} %fusion.17) | data formatting | bytes 4194304
  240.9 6.4 %all-to-all-done.1 = bf16[32,256,128]{2,1,0:T(8,128)(2,1)} async-done(((bf16[32,256,128]{2,1,0:T(8,128)(2,1)}), bf16[32,256,128]{2,1,0:T(8,128)(2,1)}, u32[]{:S(2)}, u32[]{:S(2)}) %all-to-all-start.1) | async-done | bytes 2097184 | tf_op jit(solution)/shard_map/all_to_all | solution.py:56
  247.3 4.0 %convert_bitcast_fusion = f32[256,32,128]{2,0,1:T(8,128)} fusion(bf16[32,256,128]{2,1,0:T(8,128)(2,1)} %all-to-all-done.1), kind=kLoop, calls=%fused_computation.140 | loop fusion | flops 1048576 | bytes 6291456 | tf_op jit(solution)/shard_map/convert_element_type | solution.py:69
  251.3 5.7 %copy.52 = f32[256,32,128]{0,2,1:T(8,128)} copy(f32[256,32,128]{2,0,1:T(8,128)} %convert_bitcast_fusion) | data formatting | bytes 8388608 | tf_op jit(solution)/shard_map/convert_element_type | solution.py:69
  257.0 4.8 %fusion = bf16[256,4096]{0,1:T(8,128)(2,1)} fusion(f32[256,32,128]{0,2,1:T(8,128)} %copy.52, bf16[1,256,4096]{1,2,0:T(8,128)(2,1)} %copy.47), kind=kLoop, calls=%fused_computation.19 | loop fusion | flops 3145728 | bytes 8388608 | tf_op jit(solution)/shard_map/convert_element_type | solution.py:81
  261.8 3.7 collective-permute-start.2
  265.5 4.2 %fusion.127 = bf16[1,256,4096]{1,2,0:T(8,128)(2,1)} fusion(bf16[1,256,4096]{1,2,0:T(8,128)(2,1)S(1)} %copy-done.1, bf16[256,4096]{0,1:T(8,128)(2,1)} %fusion), kind=kLoop, calls=%fused_computation.166 | loop fusion | flops 12582912 | bytes 6291456 | tf_op jit(solution)/shard_map/broadcast_in_dim | solution.py:82
  269.7 4.1 %copy.58 = bf16[1,256,4096]{2,1,0:T(8,128)(2,1)} copy(bf16[1,256,4096]{1,2,0:T(8,128)(2,1)} %fusion.127) | data formatting | bytes 4194304
  273.8 114.4 %all-gather.6.cloned.1.call-done = f32[256,1,4096]{2,1,0:T(1,128)} async-done(((f32[1,1,4096]{2,1,0:T(1,128)}), f32[256,1,4096]{2,1,0:T(1,128)}) %all-gather.6.cloned.1.call-update) | async-done | bytes 4194320 | tf_op jit(solution)/shard_map/all_gather | solution.py:83
  388.2 5.1 %reduce_sum.58 = f32[4096]{0:T(1024)} reduce(f32[256,1,4096]{2,1,0:T(1,128)} %all-gather.6.cloned.1.call-done, f32[]{:T(128)} %constant.10.clone.1), dimensions={0,1}, to_apply=%region_6.7 | reduce | flops 1044480 | bytes 4210692 | tf_op jit(solution)/shard_map/reduce_sum | solution.py:83
  393.3 1.0 copy.60
  394.3 0.5 slice_bitcast_fusion.1
  (25 shorter events, 0.2 us)
Async XLA Ops:
  7.2 81.4 %all-gather.4.cloned.1.call-start = ((), (), s32[]{:S(2)}) async-start(), calls=%async_computation.5 | async-start | bytes 2359296 | tf_op jit(solution)/shard_map/all_gather | solution.py:37
  7.2 25.4 %collective-permute-start = (bf16[128,1024]{1,0:T(8,128)(2,1)}, bf16[128,1024]{1,0:T(8,128)(2,1)S(1)}, u32[]{:S(2)}, u32[]{:S(2)}) collective-permute-start(bf16[128,1024]{1,0:T(8,128)(2,1)} %bitcast.165), channel_id=1, source_target_pairs={{0,0},{1,32},{2,64},{3,96},{4,128},{5,160},{6,192},{7,224},{32,1},... | collective-permute-start | bytes 786440 | tf_op jit(solution)/shard_map/ppermute | solution.py:27
  17.4 29.9 %copy-start = (bf16[1,256,4096]{1,2,0:T(8,128)(2,1)}, bf16[1,256,4096]{1,2,0:T(8,128)(2,1)S(1)}, u32[]{:S(2)}) copy-start(bf16[1,256,4096]{1,2,0:T(8,128)(2,1)S(1)} %copy.53) | copy-start | bytes 6291460
  32.6 0.7 copy-start.3
  51.5 33.0 %all-to-all-start.2 = ((bf16[32,256,128]{1,2,0:T(8,128)(2,1)}), bf16[32,256,128]{1,2,0:T(8,128)(2,1)}, u32[]{:S(2)}, u32[]{:S(2)}) async-start(bf16[32,256,128]{1,2,0:T(8,128)(2,1)} %bitcast.155), calls=%async_computation.2 | async-start | bytes 4194304 | tf_op jit(solution)/shard_map/all_to_all | solution.py:51
  102.5 33.5 %all-to-all-start.3 = ((bf16[32,256,128]{1,2,0:T(8,128)(2,1)}), bf16[32,256,128]{1,2,0:T(8,128)(2,1)}, u32[]{:S(2)}, u32[]{:S(2)}) async-start(bf16[32,256,128]{1,2,0:T(8,128)(2,1)} %copy.57), calls=%async_computation.3 | async-start | bytes 4194304 | tf_op jit(solution)/shard_map/all_to_all | solution.py:56
  119.4 16.6 %copy-start.4 = (f32[4096]{0:T(1024)S(1)}, f32[4096]{0:T(1024)}, u32[]{:S(2)}) copy-start(f32[4096]{0:T(1024)} %param.11) | copy-start | bytes 49156
  149.9 33.5 %all-to-all-start = ((bf16[32,256,128]{1,2,0:T(8,128)(2,1)}), bf16[32,256,128]{1,2,0:T(8,128)(2,1)}, u32[]{:S(2)}, u32[]{:S(2)}) async-start(bf16[32,256,128]{1,2,0:T(8,128)(2,1)} %fusion.121), calls=%async_computation | async-start | bytes 4194304 | tf_op jit(solution)/shard_map/all_to_all | solution.py:51
  157.4 104.5 %reduce-scatter.2.cloned.1.call-start = ((), (), s32[]{:S(2)}) async-start(), calls=%async_computation.6 | async-start | bytes 5308416 | tf_op jit(solution)/shard_map/reduce_scatter | solution.py:77
  194.5 0.8 copy-start.6
  194.6 193.6 %all-gather.6.cloned.1.call-start = ((), (), s32[]{:S(2)}) async-start(), calls=%async_computation.7 | async-start | bytes 4210688 | tf_op jit(solution)/shard_map/all_gather | solution.py:83
  195.3 9.8 %copy-start.2 = (bf16[32,256,128]{2,1,0:T(8,128)(2,1)S(1)}, bf16[32,256,128]{2,1,0:T(8,128)(2,1)}, u32[]{:S(2)}) copy-start(bf16[32,256,128]{2,1,0:T(8,128)(2,1)} %copy.49) | copy-start | bytes 6291460
  195.3 9.8 %copy-start.5 = (bf16[1024,1024]{1,0:T(8,128)(2,1)S(1)}, bf16[1024,1024]{1,0:T(8,128)(2,1)}, u32[]{:S(2)}) copy-start(bf16[1024,1024]{1,0:T(8,128)(2,1)} %all-gather.4.cloned.1.call-done) | copy-start | bytes 6291460
  195.3 9.8 %collective-permute-start.1 = (f32[1,1024]{1,0:T(1,128)S(1)}, f32[1,1024]{1,0:T(1,128)S(1)}, u32[]{:S(2)}, u32[]{:S(2)}) collective-permute-start(f32[1,1024]{1,0:T(1,128)S(1)} %copy-done.6), channel_id=1, source_target_pairs={{0,0},{1,32},{2,64},{3,96},{4,128},{5,160},{6,192},{7,224},{32,1},... | collective-permute-start | bytes 12296 | tf_op jit(solution)/shard_map/ppermute | solution.py:27
  212.7 34.5 %all-to-all-start.1 = ((bf16[32,256,128]{2,1,0:T(8,128)(2,1)}), bf16[32,256,128]{2,1,0:T(8,128)(2,1)}, u32[]{:S(2)}, u32[]{:S(2)}) async-start(bf16[32,256,128]{2,1,0:T(8,128)(2,1)} %bitcast.156), calls=%async_computation.1 | async-start | bytes 4194304 | tf_op jit(solution)/shard_map/all_to_all | solution.py:56
  257.0 8.5 %copy-start.1 = (bf16[1,256,4096]{1,2,0:T(8,128)(2,1)S(1)}, bf16[1,256,4096]{1,2,0:T(8,128)(2,1)}, u32[]{:S(2)}) copy-start(bf16[1,256,4096]{1,2,0:T(8,128)(2,1)} %copy-done) | copy-start | bytes 6291460
  261.8 131.5 %collective-permute-start.2 = (f32[128,1152]{0,1:T(8,128)}, f32[128,1152]{0,1:T(8,128)S(1)}, u32[]{:S(2)}, u32[]{:S(2)}) collective-permute-start(f32[128,1152]{0,1:T(8,128)} %reduce-scatter.2.cloned.1.call-done), channel_id=1, source_target_pairs={{0,0},{1,32},{2,64},{3,96},{4,128},{5,160},{6,192},{7,224},{32,1},... | collective-permute-start | bytes 1769480 | tf_op jit(solution)/shard_map/ppermute | solution.py:27
Sparse Core Ops, SparseCore 0:
  33.4 36.1 all-gather.3
  194.7 58.9 reduce-scatter.1
  257.9 130.2 all-gather.5
